TPU v7x, 256 devices: a whole 4x4x8 slice. The times are simulated.
256 devices in a mesh: gr: 2 (over z_hi), sp: 16 (over z_lo, y), tp: 8 (over x, core).
Axes of the slice: x: 4, y: 4, z: 8 (z_hi: 2, z_lo: 4; z = z_hi * 4 + z_lo), core: 2. Of those that a mesh axis runs over, the one named last changes fastest.
Arguments:
- tokens: bfloat16 [8, 3072, 4096], P('gr', 'sp', 'tp'), may hold values from -6.5 to 6.5
- first_token_input: bfloat16 [8, 4096], P('gr', 'sp'), may hold values from -6 to 6
- forget_weight: bfloat16 [4096, 4096], P(None, 'tp'), may hold values from -0.1171875 to 0.1171875
- value_weight: bfloat16 [4096, 4096], P(None, 'tp'), may hold values from -0.375 to 0.375
- query_weight: bfloat16 [4096, 4096], P('sp', 'tp'), may hold values from -0.09375 to 0.09375
- output_gate_weight: bfloat16 [4096, 4096], P('sp', 'tp'), may hold values from -0.09375 to 0.09375
- forget_bound_slack: float32 [4096], P('tp'), may hold values from 0.00016276042 to 0.8, as said below
- additional_damping_exponent: float32 [8, 3072, 32], P('gr', 'sp', 'tp'), may hold values from -2.2 to 0, as said below
- read_norm_scale: float32 [128], replicated, may hold values from 0.1 to 1.9
Outputs:
- cache: bfloat16 [8, 32, 128, 128], P('gr', 'tp', 'sp')
- first_read: bfloat16 [8, 4096], P('gr', 'tp')
Inputs may be any that keep to these rules, and one draw needn't show every extreme that they name: `forget_bound_slack`: positive gaps, one per channel. `additional_damping_exponent`: non-positive log-decays.
All inputs are finite; a program needn't handle non-finite values.
Results may differ from a plain program's by a relative error of at most 0.018.
Values may be sent and summed in bfloat16 or wider, within the bound.
No kernel may reach another device: no remote copies, remote signals or barrier semaphores. Data moves between devices by JAX's collectives and lax.ppermute only.
A program may use at most 64 MiB of HBM per device.

v0:
```python
import jax
import jax.numpy as jnp
from jax import lax
from jax.sharding import PartitionSpec as P


def from_everyone(shard, axis):
    count = lax.axis_size(axis)
    return lax.all_to_all(
        jnp.broadcast_to(shard[None], (count, *shard.shape)), axis, 0, 0, tiled=True
    )


def folded_in_pairs(pieces, combine):
    while len(jax.tree.leaves(pieces)[0]) > 1:
        pieces = jax.vmap(combine)(*(pieces[side::2] for side in (0, 1)))
    return pieces[0]


def prefix(shard, axis, combine, identity):
    count, position = (lax.axis_size(axis), lax.axis_index(axis))
    passed = jnp.arange(count) > position

    def kept(part, zero, own):
        part = jnp.where(
            passed.reshape(-1, *(1 for _ in own.shape)), part, jnp.asarray(zero, own.dtype)
        )
        return part[::-1]

    pieces = from_everyone(shard, axis)
    return folded_in_pairs(kept(pieces, identity, shard), combine)


def cut_along(shard, dim, count):
    shape = shard.shape
    blocks = shard.reshape(*shape[:dim], count, shape[dim] // count, *shape[dim + 1 :])
    return jnp.moveaxis(blocks, dim, 0)


def sent_and_summed(shard, axis, dim):
    count = lax.axis_size(axis)
    blocks = lax.all_to_all(cut_along(shard, dim, count), axis, 0, 0, tiled=True)
    return jnp.sum(blocks.astype(jnp.float32), axis=0)


def of_everyone(shard, axis):
    everything = from_everyone(shard, axis)
    return jnp.sum(everything, axis=0)


def packed_total(arrays, axis):
    ends = [0]
    for a in arrays:
        ends.append(ends[-1] + a.size)
    total = of_everyone(jnp.concatenate([a.ravel() for a in arrays]), axis)
    return tuple((total[b:e].reshape(a.shape) for a, b, e in zip(arrays, ends, ends[1:])))


def add_sums(earlier, later_part):
    return earlier + later_part


def per_device(
    tokens,
    first_token_input,
    forget_weight,
    value_weight,
    query_weight,
    output_gate_weight,
    forget_bound_slack,
    additional_damping_exponent,
    read_norm_scale,
):
    seq_count, block_len, width_part = tokens.shape
    head_dim = read_norm_scale.shape[0]
    local_heads = additional_damping_exponent.shape[2]
    channels = local_heads * head_dim
    flat_rows = tokens.reshape(seq_count * block_len, width_part)
    segment = lax.all_gather(flat_rows, "tp", axis=1, tiled=True)
    forget_acc = jnp.dot(segment, forget_weight, preferred_element_type=jnp.float32)
    value_acc = jnp.dot(segment, value_weight, preferred_element_type=jnp.float32)
    forget = forget_acc.astype(jnp.bfloat16).reshape(seq_count, block_len, channels)
    values = value_acc.astype(jnp.bfloat16).reshape(seq_count, block_len, local_heads, head_dim)
    sp_count = lax.axis_size("sp")
    rows_here = head_dim // sp_count
    row_start = lax.axis_index("sp") * rows_here
    valve_sampler_seeds = forget_bound_slack * jax.nn.sigmoid(-forget.astype(jnp.float32))
    damping_exponent = jnp.log1p(-valve_sampler_seeds) + jnp.repeat(
        additional_damping_exponent, head_dim, axis=2
    )
    totals = jnp.sum(damping_exponent, axis=1)
    later_sum = prefix(totals, "sp", add_sums, jnp.zeros_like(totals))
    within = totals[:, None, :] - jnp.cumsum(damping_exponent, axis=1)
    weighted = (valve_sampler_seeds * jnp.exp(within + later_sum[:, None, :])).astype(jnp.bfloat16)
    weighted = weighted.reshape(seq_count, block_len, local_heads, head_dim)
    state_terms = jnp.einsum(
        "slha,slhb->shab", weighted, values, preferred_element_type=jnp.float32
    )
    state_sum = sent_and_summed(state_terms.astype(jnp.bfloat16), "sp", 2)
    cache_rows = state_sum.astype(jnp.bfloat16)
    slab_rows = first_token_input.shape[1]
    row_first = lax.axis_index("sp") * slab_rows
    forget_rows = lax.dynamic_slice_in_dim(forget_weight, row_first, slab_rows, 0)
    value_rows = lax.dynamic_slice_in_dim(value_weight, row_first, slab_rows, 0)
    new_sums = packed_total(
        (
            jnp.dot(first_token_input, query_weight, preferred_element_type=jnp.float32),
            jnp.dot(first_token_input, output_gate_weight, preferred_element_type=jnp.float32),
            jnp.dot(first_token_input, forget_rows, preferred_element_type=jnp.float32),
            jnp.dot(first_token_input, value_rows, preferred_element_type=jnp.float32),
        ),
        "sp",
    )
    new_query, new_gate, new_forget, new_value = [
        summed.astype(jnp.bfloat16) for summed in new_sums
    ]
    new_keys = (forget_bound_slack * jax.nn.sigmoid(-new_forget.astype(jnp.float32))).reshape(
        seq_count, local_heads, head_dim
    )
    own_keys = lax.dynamic_slice_in_dim(new_keys, row_start, rows_here, 2)
    own_query = lax.dynamic_slice_in_dim(
        new_query.astype(jnp.float32).reshape(seq_count, local_heads, head_dim),
        row_start,
        rows_here,
        2,
    )
    value_new = new_value.astype(jnp.float32).reshape(seq_count, local_heads, head_dim)
    updated = (1.0 - own_keys)[..., None] * cache_rows.astype(jnp.float32) + own_keys[
        ..., None
    ] * value_new[:, :, None, :]
    read_part = jnp.einsum("sha,shab->shb", own_query, updated, precision=lax.Precision.HIGHEST)
    read_sum = of_everyone(read_part, "sp")
    scaled = (
        read_sum
        * lax.rsqrt(jnp.mean(read_sum * read_sum, axis=-1, keepdims=True) + 1e-06)
        * read_norm_scale
    )
    first_read = (
        scaled.reshape(seq_count, channels) * jax.nn.silu(new_gate.astype(jnp.float32))
    ).astype(jnp.bfloat16)
    return (cache_rows, first_read)


def solution(mesh):
    placed = (
        P("gr", "sp", "tp"),
        P("gr", "sp"),
        P(None, "tp"),
        P(None, "tp"),
        P("sp", "tp"),
        P("sp", "tp"),
        P("tp"),
        P("gr", "sp", "tp"),
        P(),
    )
    return jax.shard_map(
        per_device,
        mesh=mesh,
        in_specs=placed,
        out_specs=(P("gr", "tp", "sp", None), P("gr", "tp")),
        check_vma=False,
    )
```

profile of v0, /device:TPU:2, one launch (start us, length us, event | category | flops | bytes accessed | tf_op | source)
XLA Modules:
  0.0 156.7 jit_solution(15677566617659732985)
XLA Ops:
  7.2 0.0 copy-start
  7.2 0.0 copy-start.4
  7.2 0.0 copy-start.7
  7.2 0.0 all-gather.2.cloned.1.call-start
  7.2 0.7 all-gather.2.cloned.1.call-update
  7.9 0.2 copy-done
  8.1 0.8 convolution_bitcast_fusion.3
  8.9 1.1 convolution_bitcast_fusion.2
  10.1 1.1 convolution_bitcast_fusion.1
  11.2 0.0 copy-done.4
  11.2 1.1 convolution_bitcast_fusion
  12.3 0.0 copy-done.7
  12.3 0.2 copy.30
  12.5 0.0 copy-start.2
  12.5 1.0 broadcast_in_dim.20
  13.5 1.8 %reshape.149 = f32[4,192,512]{2,1,0:T(8,128)} reshape(f32[4,192,4,128]{3,2,1,0:T(4,128)S(1)} %broadcast_in_dim.20) | data formatting | bytes 3145728 | tf_op jit(solution)/shard_map/reshape | solution.py:88
  15.2 0.0 copy-done.2
  15.3 40.1 %all-gather.2.cloned.1.call-done = bf16[768,4096]{1,0:T(8,128)(2,1)} async-done(((bf16[768,512]{1,0:T(8,128)(2,1)}), bf16[768,4096]{1,0:T(8,128)(2,1)}) %all-gather.2.cloned.1.call-update) | async-done | bytes 6291472 | tf_op jit(solution)/shard_map/all_gather | solution.py:79
  55.3 7.4 %convolution_convert_fusion = bf16[768,512]{1,0:T(8,128)(2,1)S(1)} fusion(bf16[768,4096]{1,0:T(8,128)(2,1)} %all-gather.2.cloned.1.call-done, bf16[4096,512]{1,0:T(8,128)(2,1)} %param.12), kind=kOutput, calls=%fused_computation.10 | convolution fusion | flops 3221618688 | bytes 11272192 | tf_op jit(solution)/shard_map/dot_general | solution.py:81
  62.7 1.1 reshape.153
  63.9 7.0 %add_divide_fusion = f32[768,512]{1,0:T(8,128)S(1)} fusion(bf16[768,4096]{1,0:T(8,128)(2,1)} %all-gather.2.cloned.1.call-done, bf16[4096,512]{1,0:T(8,128)(2,1)} %param.11), kind=kOutput, calls=%fused_computation.9 | convolution fusion | flops 3222798336 | bytes 12058624 | tf_op jit(solution)/shard_map/dot_general | solution.py:80
  70.8 0.0 copy-start.5
  70.8 0.5 div.22
  71.4 0.1 copy-done.5
  71.5 2.4 %add_reduce_fusion = f32[4,4,128]{2,1,0:T(4,128)S(1)} fusion(f32[4,192,4,128]{3,2,1,0:T(4,128)S(1)} %div.22, f32[4,192,4]{2,1,0:T(8,128)} %copy-done.2, f32[4,128]{1,0:T(4,128)S(1)} %bitcast.77), kind=kLoop, calls=%fused_computation.8 | loop fusion | flops 1570816 | bytes 1595392 | tf_op jit(solution)/shard_map/reduce_sum | solution.py:91
  73.9 0.7 broadcast_in_dim.22
  74.6 7.4 %all-to-all-start = ((f32[16,4,512]{2,1,0:T(4,128)}), f32[16,4,512]{2,1,0:T(4,128)S(1)}, u32[]{:S(2)}, u32[]{:S(2)}) async-start(f32[16,4,512]{2,1,0:T(4,128)} %broadcast_in_dim.22), calls=%async_computation | async-start | bytes 262144 | tf_op jit(solution)/shard_map/all_to_all | solution.py:9
  82.0 2.0 %add_bitcast_fusion = f32[4,512,192]{1,2,0:T(8,128)S(1)} fusion(f32[4,192,512]{2,1,0:T(8,128)} %reshape.149, f32[4,192,512]{2,1,0:T(8,128)S(1)} %bitcast.70, f32[512]{0:T(512)S(1)} %copy-done.5), kind=kLoop, calls=%fused_computation.7 | loop fusion | flops 1179648 | bytes 4720640 | tf_op jit(solution)/shard_map/transpose
  84.0 0.3 pad.3
  84.3 1.6 %fusion = f32[4,512,2,128]{1,2,3,0:T(2,128)S(1)} fusion(f32[4,512,2,128]{1,3,2,0:T(8,128)S(1)} %bitcast.72), kind=kOutput, calls=%fused_computation | output fusion | flops 66584576 | bytes 4194304 | tf_op jit(solution)/shard_map/reduce-window
  85.9 0.0 copy-start.1
  85.9 1.3 copy-done.1
  87.3 0.1 reduce-window.9
  87.3 2.3 %broadcast_add_fusion = f32[4,512,2,128]{1,2,3,0:T(2,128)S(1)} fusion(f32[4,512,2,128]{1,2,3,0:T(2,128)} %copy-done.1, f32[4,512,2]{1,2,0:T(2,128)S(1)} %slice.107), kind=kLoop, calls=%fused_computation.18 | loop fusion | flops 524288 | bytes 4210688 | tf_op jit(solution)/shard_map/reduce_window_sum
  89.7 1.7 %copy.32 = f32[4,512,2,128]{1,3,2,0:T(8,128)} copy(f32[4,512,2,128]{1,2,3,0:T(2,128)S(1)} %broadcast_add_fusion) | data formatting | bytes 4194304 | tf_op jit(solution)/shard_map/reduce_window_sum
  91.4 0.0 copy-start.3
  91.4 0.0 all-to-all-done
  91.4 1.2 broadcast_in_dim.24
  92.6 7.5 %all-to-all-start.2 = ((f32[16,1,8192]{2,1,0:T(1,128)}), f32[16,1,8192]{2,1,0:T(1,128)S(1)}, u32[]{:S(2)}, u32[]{:S(2)}) async-start(f32[16,1,8192]{2,1,0:T(1,128)} %broadcast_in_dim.24), calls=%async_computation.2 | async-start | bytes 1048576 | tf_op jit(solution)/shard_map/all_to_all | solution.py:9
  100.1 0.1 broadcast_select_fusion
  100.3 0.0 copy-done.3
  100.3 2.1 %fusion.6 = bf16[4,4,16,8,128]{4,3,2,1,0:T(8,128)(2,1)S(1)} fusion(bf16[4,192,4,128]{3,2,1,0:T(4,128)(2,1)S(1)} %copy-done.3, f32[4,256,512]{2,1,0:T(8,128)} %bitcast.73, f32[4,192,512]{2,1,0:T(8,128)S(1)} %bitcast.71, f32[4,512]{1,0:T(4,128)S(1)} %fusion.22, f32[4,512]{1,0:T(4,128)S(1)} %bitcast.76, f32[512]{0:T(512)S(1)} %copy-done.5), kind=kOutput, calls=%fused_computation.13 | convolution fusion | flops 102891520 | bytes 4474880 | tf_op jit(solution)/shard_map/slha,slhb->shab/dot_general | solution.py:96
  102.4 0.9 copy.64
  103.3 12.0 %all-to-all-done.2 = f32[16,1,8192]{2,1,0:T(1,128)S(1)} async-done(((f32[16,1,8192]{2,1,0:T(1,128)}), f32[16,1,8192]{2,1,0:T(1,128)S(1)}, u32[]{:S(2)}, u32[]{:S(2)}) %all-to-all-start.2) | async-done | bytes 524320 | tf_op jit(solution)/shard_map/all_to_all | solution.py:9
  115.3 0.0 copy-start.8
  115.3 4.6 %all-to-all-start.1 = ((bf16[16,4,4,8,128]{4,3,2,1,0:T(8,128)(2,1)}), bf16[16,4,4,8,128]{4,3,2,1,0:T(8,128)(2,1)S(1)}, u32[]{:S(2)}, u32[]{:S(2)}) async-start(bf16[16,4,4,8,128]{4,3,2,1,0:T(8,128)(2,1)} %bitcast.68), calls=%async_computation.1 | async-start | bytes 1048576 | tf_op jit(solution)/shard_map/all_to_all | solution.py:42
  120.0 0.4 reduce_sum.50
  120.5 0.1 dynamic-slice_bitcast_fusion
  120.5 0.1 broadcast_subtract_fusion
  120.6 14.1 %all-to-all-done.1 = bf16[16,4,4,8,128]{4,3,2,1,0:T(8,128)(2,1)S(1)} async-done(((bf16[16,4,4,8,128]{4,3,2,1,0:T(8,128)(2,1)}), bf16[16,4,4,8,128]{4,3,2,1,0:T(8,128)(2,1)S(1)}, u32[]{:S(2)}, u32[]{:S(2)}) %all-to-all-start.1) | async-done | bytes 524320 | tf_op jit(solution)/shard_map/all_to_all | solution.py:42
  134.7 0.1 reduce_sum.49
  134.8 0.0 copy-start.6
  134.8 0.3 fusion.13
  135.0 0.7 broadcast_in_dim.25
  135.7 4.4 %all-to-all-start.3 = ((f32[16,4,4,128]{3,2,1,0:T(4,128)}), f32[16,4,4,128]{3,2,1,0:T(4,128)S(1)}, u32[]{:S(2)}, u32[]{:S(2)}) async-start(f32[16,4,4,128]{3,2,1,0:T(4,128)} %broadcast_in_dim.25), calls=%async_computation.3 | async-start | bytes 262144 | tf_op jit(solution)/shard_map/all_to_all | solution.py:9
  140.1 0.0 copy-done.8
  140.2 8.9 %all-to-all-done.3 = f32[16,4,4,128]{3,2,1,0:T(4,128)S(1)} async-done(((f32[16,4,4,128]{3,2,1,0:T(4,128)}), f32[16,4,4,128]{3,2,1,0:T(4,128)S(1)}, u32[]{:S(2)}, u32[]{:S(2)}) %all-to-all-start.3) | async-done | bytes 131104 | tf_op jit(solution)/shard_map/all_to_all | solution.py:9
  149.1 0.1 multiply_reduce_fusion
  149.2 0.1 multiply_bitcast_fusion
  149.3 0.6 fusion.24
  149.9 0.0 copy-done.6
  (24 shorter events, 0.2 us)
Async XLA Ops:
  7.2 1.0 copy-start
  7.2 4.0 %copy-start.4 = (bf16[4,256]{1,0:T(4,128)(2,1)S(1)}, bf16[4,256]{1,0:T(4,128)(2,1)}, u32[]{:S(2)}) copy-start(bf16[4,256]{1,0:T(4,128)(2,1)} %param.10) | copy-start | bytes 6148
  7.2 5.1 %copy-start.7 = (f32[4,192,4]{1,2,0:T(4,128)S(1)}, f32[4,192,4]{1,2,0:T(4,128)}, u32[]{:S(2)}) copy-start(f32[4,192,4]{1,2,0:T(4,128)} %param.16) | copy-start | bytes 36868
  7.2 48.1 %all-gather.2.cloned.1.call-start = ((), (), s32[]{:S(2)}) async-start(), calls=%async_computation.4 | async-start | bytes 7077888 | tf_op jit(solution)/shard_map/all_gather | solution.py:79
  12.5 2.8 %copy-start.2 = (f32[4,192,4]{2,1,0:T(8,128)}, f32[4,192,4]{2,1,0:T(8,128)S(1)}, u32[]{:S(2)}) copy-start(f32[4,192,4]{2,1,0:T(8,128)S(1)} %copy.30) | copy-start | bytes 36868
  70.8 0.7 copy-start.5
  74.6 16.8 %all-to-all-start = ((f32[16,4,512]{2,1,0:T(4,128)}), f32[16,4,512]{2,1,0:T(4,128)S(1)}, u32[]{:S(2)}, u32[]{:S(2)}) async-start(f32[16,4,512]{2,1,0:T(4,128)} %broadcast_in_dim.22), calls=%async_computation | async-start | bytes 262144 | tf_op jit(solution)/shard_map/all_to_all | solution.py:9
  85.9 1.3 copy-start.1
  91.4 8.9 %copy-start.3 = (bf16[4,192,4,128]{3,2,1,0:T(4,128)(2,1)S(1)}, bf16[4,192,4,128]{3,2,1,0:T(4,128)(2,1)}, u32[]{:S(2)}) copy-start(bf16[4,192,4,128]{3,2,1,0:T(4,128)(2,1)} %reshape.153) | copy-start | bytes 2359300
  92.6 22.8 %all-to-all-start.2 = ((f32[16,1,8192]{2,1,0:T(1,128)}), f32[16,1,8192]{2,1,0:T(1,128)S(1)}, u32[]{:S(2)}, u32[]{:S(2)}) async-start(f32[16,1,8192]{2,1,0:T(1,128)} %broadcast_in_dim.24), calls=%async_computation.2 | async-start | bytes 1048576 | tf_op jit(solution)/shard_map/all_to_all | solution.py:9
  115.3 24.8 %copy-start.8 = (f32[128]{0:T(128)S(1)}, f32[128]{0:T(128)}, u32[]{:S(2)}) copy-start(f32[128]{0:T(128)} %param.17) | copy-start | bytes 1540
  115.3 19.3 %all-to-all-start.1 = ((bf16[16,4,4,8,128]{4,3,2,1,0:T(8,128)(2,1)}), bf16[16,4,4,8,128]{4,3,2,1,0:T(8,128)(2,1)S(1)}, u32[]{:S(2)}, u32[]{:S(2)}) async-start(bf16[16,4,4,8,128]{4,3,2,1,0:T(8,128)(2,1)} %bitcast.68), calls=%async_computation.1 | async-start | bytes 1048576 | tf_op jit(solution)/shard_map/all_to_all | solution.py:42
  134.8 15.1 %copy-start.6 = (bf16[4,4,8,128]{3,2,1,0:T(8,128)(2,1)}, bf16[4,4,8,128]{3,2,1,0:T(8,128)(2,1)S(1)}, u32[]{:S(2)}) copy-start(bf16[4,4,8,128]{3,2,1,0:T(8,128)(2,1)S(1)} %reduce_sum.49) | copy-start | bytes 98308
  135.7 13.4 %all-to-all-start.3 = ((f32[16,4,4,128]{3,2,1,0:T(4,128)}), f32[16,4,4,128]{3,2,1,0:T(4,128)S(1)}, u32[]{:S(2)}, u32[]{:S(2)}) async-start(f32[16,4,4,128]{3,2,1,0:T(4,128)} %broadcast_in_dim.25), calls=%async_computation.3 | async-start | bytes 262144 | tf_op jit(solution)/shard_map/all_to_all | solution.py:9
Sparse Core Ops, SparseCore 0:
  9.8 45.4 all-gather.1
where the time goes:
time: 157 us
  waiting for transfers between devices  75.7 us (48%)
  starting transfers between devices  24 us (15%)
  matrix products  20.8 us (13%)
  between operations  14.3 us (9%)
  local copies, waits for them, and re-layouts  11.9 us (8%)
  other arithmetic  10 us (6%)
    all_gather x1, waiting for transfers between devices, per_device(): segment = lax.all_gather(flat_rows, 'tp', axis=1, tiled=True)  40.1 us
    all_to_all x3, waiting for transfers between devices, from_everyone(): lax.all_to_all(jnp.broadcast_to(shard[None], (count, *shard.shape)), axis...  20.9 us
    all_to_all x3, starting transfers between devices, from_everyone(): lax.all_to_all(jnp.broadcast_to(shard[None], (count, *shard.shape)), axis...  19.3 us
    all_to_all x1, waiting for transfers between devices, sent_and_summed(): lax.all_to_all(cut_along(shard, dim, count), axis, 0, 0, tiled=True)  14.1 us
    dot_general x1, matrix products, per_device(): jnp.dot(segment, value_weight, preferred_element_type=jnp.float32)  7.4 us
    dot_general x1, matrix products, per_device(): jnp.dot(segment, forget_weight, preferred_element_type=jnp.float32)  6.97 us
    all_to_all x1, starting transfers between devices, sent_and_summed(): lax.all_to_all(cut_along(shard, dim, count), axis, 0, 0, tiled=True)  4.63 us
    another operation x3, other arithmetic  4.02 us
  transfers between devices with their start and end apart: 5, of which 4 were waited for; matrix products, arithmetic and copies ran while one was open for 12% of the time, Pallas kernels for 0%

commit v1 on v0

--- a/solution.py
+++ b/solution.py
@@ -76,7 +76,19 @@
     local_heads = additional_damping_exponent.shape[2]
     channels = local_heads * head_dim
     flat_rows = tokens.reshape(seq_count * block_len, width_part)
-    segment = lax.all_gather(flat_rows, "tp", axis=1, tiled=True)
+    u_in = flat_rows
+    value_now, mixed_arr, far_arr = (lax.axis_size("tp"), lax.axis_index("tp"), u_in.shape[1])
+    line_up = [d * value_now if i0 == 1 else d for i0, d in enumerate(u_in.shape)]
+    segment = lax.dynamic_update_slice_in_dim(
+        jnp.zeros(line_up, u_in.dtype), u_in, mixed_arr * far_arr, axis=1
+    )
+    nth = 1
+    while nth < value_now:
+        u_in = lax.ppermute(u_in, "tp", [(i0, (i0 + 1) % value_now) for i0 in range(value_now)])
+        segment = lax.dynamic_update_slice_in_dim(
+            segment, u_in, (mixed_arr - nth) % value_now * far_arr, axis=1
+        )
+        nth += 1
     forget_acc = jnp.dot(segment, forget_weight, preferred_element_type=jnp.float32)
     value_acc = jnp.dot(segment, value_weight, preferred_element_type=jnp.float32)
     forget = forget_acc.astype(jnp.bfloat16).reshape(seq_count, block_len, channels)

time: 157 us -> 179 us (1.14)
  the two profiles are of different devices: /device:TPU:2 before, /device:TPU:8 now
where the time goes in v1:
time: 179 us; the launch traced here: 178 us
  waiting for transfers between devices  105 us (59%)
  starting transfers between devices  30 us (17%)
  local copies, waits for them, and re-layouts  18.4 us (10%)
  matrix products  12.8 us (7%)
  other arithmetic  10.6 us (6%)
    ppermute x7, waiting for transfers between devices, per_device(): lax.ppermute(u_in, 'tp', [(i0, (i0 + 1) % value_now) for i0 in range(valu...  77.9 us
    all_to_all x3, starting transfers between devices, from_everyone(): lax.all_to_all(jnp.broadcast_to(shard[None], (count, *shard.shape)), axis...  21.7 us
    all_to_all x3, waiting for transfers between devices, from_everyone(): lax.all_to_all(jnp.broadcast_to(shard[None], (count, *shard.shape)), axis...  15.9 us
    all_to_all x1, waiting for transfers between devices, sent_and_summed(): lax.all_to_all(cut_along(shard, dim, count), axis, 0, 0, tiled=True)  11.3 us
    all_to_all x1, starting transfers between devices, sent_and_summed(): lax.all_to_all(cut_along(shard, dim, count), axis, 0, 0, tiled=True)  8.25 us
    unnamed x38, local copies, waits for them, and re-layouts  4.57 us
    dot_general x1, matrix products, per_device(): jnp.dot(segment, value_weight, preferred_element_type=jnp.float32)  4.35 us
    another operation x3, other arithmetic  4.01 us
  transfers between devices with their start and end apart: 11, of which 10 were waited for; matrix products, arithmetic and copies ran while one was open for 13% of the time, Pallas kernels for 0%

profile of v1, /device:TPU:8, one launch (start us, length us, event | category | flops | bytes accessed | tf_op | source)
XLA Modules:
  0.0 178.0 jit_solution(2939625602254514372)
XLA Ops:
  0.6 0.0 copy-start
  0.6 0.0 collective-permute-start
  0.7 12.8 %collective-permute-done = bf16[768,512]{1,0:T(8,128)(2,1)S(1)} collective-permute-done((bf16[768,512]{1,0:T(8,128)(2,1)}, bf16[768,512]{1,0:T(8,128)(2,1)S(1)}, u32[]{:S(2)}, u32[]{:S(2)}) %collective-permute-start) | collective-permute-done | bytes 786464 | tf_op jit(solution)/shard_map/ppermute | solution.py:87
  13.5 12.6 %collective-permute-done.1 = bf16[768,512]{1,0:T(8,128)(2,1)S(1)} collective-permute-done((bf16[768,512]{1,0:T(8,128)(2,1)S(1)}, bf16[768,512]{1,0:T(8,128)(2,1)S(1)}, u32[]{:S(2)}, u32[]{:S(2)}) %collective-permute-start.1) | collective-permute-done | bytes 786464 | tf_op jit(solution)/shard_map/ppermute | solution.py:87
  26.1 0.9 copy-done.4
  27.0 12.6 %collective-permute-done.2 = bf16[768,512]{1,0:T(8,128)(2,1)S(1)} collective-permute-done((bf16[768,512]{1,0:T(8,128)(2,1)S(1)}, bf16[768,512]{1,0:T(8,128)(2,1)S(1)}, u32[]{:S(2)}, u32[]{:S(2)}) %collective-permute-start.2) | collective-permute-done | bytes 786464 | tf_op jit(solution)/shard_map/ppermute | solution.py:87
  39.6 0.9 copy-done.6
  40.5 12.7 %collective-permute-done.3 = bf16[768,512]{1,0:T(8,128)(2,1)} collective-permute-done((bf16[768,512]{1,0:T(8,128)(2,1)S(1)}, bf16[768,512]{1,0:T(8,128)(2,1)}, u32[]{:S(2)}, u32[]{:S(2)}) %collective-permute-start.3) | collective-permute-done | bytes 786464 | tf_op jit(solution)/shard_map/ppermute | solution.py:87
  53.2 0.9 copy.30
  54.2 0.0 copy-start.10
  54.2 1.0 broadcast_in_dim.23
  55.2 1.8 %reshape.149 = f32[4,192,512]{2,1,0:T(8,128)} reshape(f32[4,192,4,128]{3,2,1,0:T(4,128)S(1)} %broadcast_in_dim.23) | data formatting | bytes 3145728 | tf_op jit(solution)/shard_map/reshape | solution.py:100
  56.9 9.2 %collective-permute-done.4 = bf16[768,512]{1,0:T(8,128)(2,1)} collective-permute-done((bf16[768,512]{1,0:T(8,128)(2,1)}, bf16[768,512]{1,0:T(8,128)(2,1)}, u32[]{:S(2)}, u32[]{:S(2)}) %collective-permute-start.4) | collective-permute-done | bytes 786464 | tf_op jit(solution)/shard_map/ppermute | solution.py:87
  66.2 1.1 convolution_bitcast_fusion.1
  67.3 1.1 convolution_bitcast_fusion
  68.4 0.1 convolution_bitcast_fusion.3
  68.5 0.1 convolution_bitcast_fusion.2
  68.7 0.6 pad_maximum_fusion
  69.3 0.8 broadcast_in_dim.22
  70.1 0.4 copy-done.3
  70.5 0.1 constant_dynamic-update-slice_fusion.7
  70.6 8.4 %collective-permute-done.5 = bf16[768,512]{1,0:T(8,128)(2,1)S(1)} collective-permute-done((bf16[768,512]{1,0:T(8,128)(2,1)}, bf16[768,512]{1,0:T(8,128)(2,1)S(1)}, u32[]{:S(2)}, u32[]{:S(2)}) %collective-permute-start.5) | collective-permute-done | bytes 786464 | tf_op jit(solution)/shard_map/ppermute | solution.py:87
  79.0 0.1 constant_dynamic-update-slice_fusion.6
  79.1 0.1 constant_dynamic-update-slice_fusion.5
  79.3 0.1 constant_dynamic-update-slice_fusion.4
  79.4 1.2 constant_dynamic-update-slice_fusion.3
  80.6 1.4 constant_dynamic-update-slice_fusion.2
  82.0 0.1 constant_dynamic-update-slice_fusion.1
  82.2 9.5 %collective-permute-done.6 = bf16[768,512]{1,0:T(8,128)(2,1)S(1)} collective-permute-done((bf16[768,512]{1,0:T(8,128)(2,1)S(1)}, bf16[768,512]{1,0:T(8,128)(2,1)S(1)}, u32[]{:S(2)}, u32[]{:S(2)}) %collective-permute-start.6) | collective-permute-done | bytes 786464 | tf_op jit(solution)/shard_map/ppermute | solution.py:87
  91.6 0.1 constant_dynamic-update-slice_fusion
  91.8 3.6 %add_divide_fusion = f32[768,512]{1,0:T(8,128)S(1)} fusion(bf16[768,4096]{1,0:T(8,128)(2,1)S(1)} %constant_dynamic-update-slice_fusion, bf16[4096,512]{1,0:T(8,128)(2,1)S(1)} %copy-done.13), kind=kOutput, calls=%fused_computation.9 | convolution fusion | flops 3222798336 | bytes 12058624 | tf_op jit(solution)/shard_map/dot_general | solution.py:92
  95.4 4.4 %convolution_convert_fusion = bf16[768,512]{1,0:T(8,128)(2,1)} fusion(bf16[768,4096]{1,0:T(8,128)(2,1)S(1)} %constant_dynamic-update-slice_fusion, bf16[4096,512]{1,0:T(8,128)(2,1)S(1)} %copy-done.14), kind=kOutput, calls=%fused_computation.10 | convolution fusion | flops 3221618688 | bytes 11272192 | tf_op jit(solution)/shard_map/dot_general | solution.py:93
  99.8 0.5 div.22
  100.3 0.1 copy-done.11
  100.5 2.4 %add_reduce_fusion = f32[4,4,128]{2,1,0:T(4,128)S(1)} fusion(f32[4,192,4,128]{3,2,1,0:T(4,128)S(1)} %div.22, f32[4,192,4]{2,1,0:T(8,128)} %copy-done.2, f32[4,128]{1,0:T(4,128)S(1)} %bitcast.78), kind=kLoop, calls=%fused_computation.8 | loop fusion | flops 1570816 | bytes 1595392 | tf_op jit(solution)/shard_map/reduce_sum | solution.py:103
  102.9 0.7 broadcast_in_dim.25
  103.6 9.0 %all-to-all-start = ((f32[16,4,512]{2,1,0:T(4,128)}), f32[16,4,512]{2,1,0:T(4,128)S(1)}, u32[]{:S(2)}, u32[]{:S(2)}) async-start(f32[16,4,512]{2,1,0:T(4,128)} %broadcast_in_dim.25), calls=%async_computation | async-start | bytes 262144 | tf_op jit(solution)/shard_map/all_to_all | solution.py:9
  112.5 2.0 %add_bitcast_fusion = f32[4,512,192]{1,2,0:T(8,128)S(1)} fusion(f32[4,192,512]{2,1,0:T(8,128)} %reshape.149, f32[4,192,512]{2,1,0:T(8,128)S(1)} %bitcast.70, f32[512]{0:T(512)S(1)} %copy-done.11), kind=kLoop, calls=%fused_computation.7 | loop fusion | flops 1179648 | bytes 4720640 | tf_op jit(solution)/shard_map/transpose
  114.6 0.3 pad.3
  114.8 1.6 fusion
  116.5 1.3 copy-done.1
  117.8 0.1 reduce-window.9
  117.9 2.3 %broadcast_add_fusion = f32[4,512,2,128]{1,2,3,0:T(2,128)S(1)} fusion(f32[4,512,2,128]{1,2,3,0:T(2,128)} %copy-done.1, f32[4,512,2]{1,2,0:T(2,128)S(1)} %slice.107), kind=kLoop, calls=%fused_computation.18 | loop fusion | flops 524288 | bytes 4210688 | tf_op jit(solution)/shard_map/reduce_window_sum
  120.2 1.7 copy.32
  121.9 0.2 reshape.153
  122.1 2.0 %broadcast_in_dim.27 = f32[16,1,8192]{2,1,0:T(1,128)} broadcast(f32[8192]{0:T(1024)} %pad_maximum_fusion), dimensions={2} | broadcast | bytes 557056 | tf_op jit(solution)/shard_map/broadcast_in_dim | solution.py:10
  124.1 7.5 %all-to-all-start.2 = ((f32[16,1,8192]{2,1,0:T(1,128)}), f32[16,1,8192]{2,1,0:T(1,128)S(1)}, u32[]{:S(2)}, u32[]{:S(2)}) async-start(f32[16,1,8192]{2,1,0:T(1,128)} %broadcast_in_dim.27), calls=%async_computation.2 | async-start | bytes 1048576 | tf_op jit(solution)/shard_map/all_to_all | solution.py:9
  131.6 0.1 broadcast_select_fusion
  131.8 2.1 %fusion.6 = bf16[4,4,16,8,128]{4,3,2,1,0:T(8,128)(2,1)S(1)} fusion(bf16[4,192,4,128]{3,2,1,0:T(4,128)(2,1)S(1)} %reshape.153, f32[4,256,512]{2,1,0:T(8,128)} %bitcast.73, f32[4,192,512]{2,1,0:T(8,128)S(1)} %bitcast.71, f32[4,512]{1,0:T(4,128)S(1)} %fusion.22, f32[4,512]{1,0:T(4,128)S(1)} %bitcast.77, f32[512]{0:T(512)S(1)} %copy-done.11), kind=kOutput, calls=%fused_computation.13 | convolution fusion | flops 102891520 | bytes 4474880 | tf_op jit(solution)/shard_map/slha,slhb->shab/dot_general | solution.py:108
  133.9 0.9 copy.64
  134.8 8.4 %all-to-all-done.2 = f32[16,1,8192]{2,1,0:T(1,128)S(1)} async-done(((f32[16,1,8192]{2,1,0:T(1,128)}), f32[16,1,8192]{2,1,0:T(1,128)S(1)}, u32[]{:S(2)}, u32[]{:S(2)}) %all-to-all-start.2) | async-done | bytes 524320 | tf_op jit(solution)/shard_map/all_to_all | solution.py:9
  143.2 8.2 %all-to-all-start.1 = ((bf16[16,4,4,8,128]{4,3,2,1,0:T(8,128)(2,1)}), bf16[16,4,4,8,128]{4,3,2,1,0:T(8,128)(2,1)S(1)}, u32[]{:S(2)}, u32[]{:S(2)}) async-start(bf16[16,4,4,8,128]{4,3,2,1,0:T(8,128)(2,1)} %bitcast.68), calls=%async_computation.1 | async-start | bytes 1048576 | tf_op jit(solution)/shard_map/all_to_all | solution.py:42
  151.5 0.4 reduce_sum.50
  151.9 0.1 dynamic-slice_bitcast_fusion
  152.0 0.1 broadcast_subtract_fusion
  152.1 11.3 %all-to-all-done.1 = bf16[16,4,4,8,128]{4,3,2,1,0:T(8,128)(2,1)S(1)} async-done(((bf16[16,4,4,8,128]{4,3,2,1,0:T(8,128)(2,1)}), bf16[16,4,4,8,128]{4,3,2,1,0:T(8,128)(2,1)S(1)}, u32[]{:S(2)}, u32[]{:S(2)}) %all-to-all-start.1) | async-done | bytes 524320 | tf_op jit(solution)/shard_map/all_to_all | solution.py:42
  163.4 0.1 reduce_sum.49
  163.5 0.3 fusion.13
  163.7 0.7 broadcast_in_dim.28
  164.4 5.2 %all-to-all-start.3 = ((f32[16,4,4,128]{3,2,1,0:T(4,128)}), f32[16,4,4,128]{3,2,1,0:T(4,128)S(1)}, u32[]{:S(2)}, u32[]{:S(2)}) async-start(f32[16,4,4,128]{3,2,1,0:T(4,128)} %broadcast_in_dim.28), calls=%async_computation.3 | async-start | bytes 262144 | tf_op jit(solution)/shard_map/all_to_all | solution.py:9
  169.6 7.5 %all-to-all-done.3 = f32[16,4,4,128]{3,2,1,0:T(4,128)S(1)} async-done(((f32[16,4,4,128]{3,2,1,0:T(4,128)}), f32[16,4,4,128]{3,2,1,0:T(4,128)S(1)}, u32[]{:S(2)}, u32[]{:S(2)}) %all-to-all-start.3) | async-done | bytes 131104 | tf_op jit(solution)/shard_map/all_to_all | solution.py:9
  177.2 0.1 multiply_reduce_fusion
  177.3 0.1 multiply_bitcast_fusion
  177.4 0.6 fusion.24
  (55 shorter events, 0.3 us)
Async XLA Ops:
  0.6 67.8 %copy-start = (bf16[256,512]{1,0:T(8,128)(2,1)S(1)}, bf16[256,512]{1,0:T(8,128)(2,1)}, u32[]{:S(2)}) copy-start(bf16[256,512]{1,0:T(8,128)(2,1)} %param.13) | copy-start | bytes 786436
  0.6 12.8 %collective-permute-start = (bf16[768,512]{1,0:T(8,128)(2,1)}, bf16[768,512]{1,0:T(8,128)(2,1)S(1)}, u32[]{:S(2)}, u32[]{:S(2)}) collective-permute-start(bf16[768,512]{1,0:T(8,128)(2,1)} %bitcast.74), channel_id=1, source_target_pairs={{0,1},{1,2},{2,3},{3,4},{4,5},{5,6},{6,7},{7,0},{8,9},{9,10},{10,1... | collective-permute-start | bytes 2359304 | tf_op jit(solution)/shard_map/ppermute | solution.py:87
  13.5 12.6 %collective-permute-start.1 = (bf16[768,512]{1,0:T(8,128)(2,1)S(1)}, bf16[768,512]{1,0:T(8,128)(2,1)S(1)}, u32[]{:S(2)}, u32[]{:S(2)}) collective-permute-start(bf16[768,512]{1,0:T(8,128)(2,1)S(1)} %collective-permute-done), channel_id=1, source_target_pairs={{0,1},{1,2},{2,3},{3,4},{4,5},{5,6},{6,7},{7,0},{8,9},{9,10},{10,1... | collective-permute-start | bytes 2359304 | tf_op jit(solution)/shard_map/ppermute | solution.py:87
  26.1 0.9 copy-start.4
  27.0 12.6 %collective-permute-start.2 = (bf16[768,512]{1,0:T(8,128)(2,1)S(1)}, bf16[768,512]{1,0:T(8,128)(2,1)S(1)}, u32[]{:S(2)}, u32[]{:S(2)}) collective-permute-start(bf16[768,512]{1,0:T(8,128)(2,1)S(1)} %collective-permute-done.1), channel_id=1, source_target_pairs={{0,1},{1,2},{2,3},{3,4},{4,5},{5,6},{6,7},{7,0},{8,9},{9,10},{10,1... | collective-permute-start | bytes 2359304 | tf_op jit(solution)/shard_map/ppermute | solution.py:87
  39.6 0.9 copy-start.6
  40.5 12.7 %collective-permute-start.3 = (bf16[768,512]{1,0:T(8,128)(2,1)S(1)}, bf16[768,512]{1,0:T(8,128)(2,1)}, u32[]{:S(2)}, u32[]{:S(2)}) collective-permute-start(bf16[768,512]{1,0:T(8,128)(2,1)S(1)} %collective-permute-done.2), channel_id=1, source_target_pairs={{0,1},{1,2},{2,3},{3,4},{4,5},{5,6},{6,7},{7,0},{8,9},{9,10},{10,1... | collective-permute-start | bytes 2359304 | tf_op jit(solution)/shard_map/ppermute | solution.py:87
  53.2 12.9 %collective-permute-start.4 = (bf16[768,512]{1,0:T(8,128)(2,1)}, bf16[768,512]{1,0:T(8,128)(2,1)}, u32[]{:S(2)}, u32[]{:S(2)}) collective-permute-start(bf16[768,512]{1,0:T(8,128)(2,1)} %collective-permute-done.3), channel_id=1, source_target_pairs={{0,1},{1,2},{2,3},{3,4},{4,5},{5,6},{6,7},{7,0},{8,9},{9,10},{10,1... | collective-permute-start | bytes 2359304 | tf_op jit(solution)/shard_map/ppermute | solution.py:87
  54.1 2.8 %copy-start.2 = (f32[4,192,4]{2,1,0:T(8,128)}, f32[4,192,4]{2,1,0:T(8,128)S(1)}, u32[]{:S(2)}) copy-start(f32[4,192,4]{2,1,0:T(8,128)S(1)} %copy.30) | copy-start | bytes 36868
  54.2 12.0 %copy-start.10 = (bf16[4,256]{1,0:T(4,128)(2,1)S(1)}, bf16[4,256]{1,0:T(4,128)(2,1)}, u32[]{:S(2)}) copy-start(bf16[4,256]{1,0:T(4,128)(2,1)} %param.10) | copy-start | bytes 6148
  55.1 13.4 %copy-start.9 = (bf16[256,512]{1,0:T(8,128)(2,1)S(1)}, bf16[256,512]{1,0:T(8,128)(2,1)}, u32[]{:S(2)}) copy-start(bf16[256,512]{1,0:T(8,128)(2,1)} %param.14) | copy-start | bytes 786436
  66.2 12.8 %collective-permute-start.5 = (bf16[768,512]{1,0:T(8,128)(2,1)}, bf16[768,512]{1,0:T(8,128)(2,1)S(1)}, u32[]{:S(2)}, u32[]{:S(2)}) collective-permute-start(bf16[768,512]{1,0:T(8,128)(2,1)} %collective-permute-done.4), channel_id=1, source_target_pairs={{0,1},{1,2},{2,3},{3,4},{4,5},{5,6},{6,7},{7,0},{8,9},{9,10},{10,1... | collective-permute-start | bytes 2359304 | tf_op jit(solution)/shard_map/ppermute | solution.py:87
  69.3 1.1 copy-start.3
  70.5 8.7 %copy-start.5 = (bf16[768,512]{1,0:T(8,128)(2,1)S(1)}, bf16[768,512]{1,0:T(8,128)(2,1)}, u32[]{:S(2)}) copy-start(bf16[768,512]{1,0:T(8,128)(2,1)} %copy-done.4) | copy-start | bytes 2359300
  70.5 8.8 %copy-start.7 = (bf16[768,512]{1,0:T(8,128)(2,1)S(1)}, bf16[768,512]{1,0:T(8,128)(2,1)}, u32[]{:S(2)}) copy-start(bf16[768,512]{1,0:T(8,128)(2,1)} %copy-done.6) | copy-start | bytes 2359300
  79.0 12.6 %collective-permute-start.6 = (bf16[768,512]{1,0:T(8,128)(2,1)S(1)}, bf16[768,512]{1,0:T(8,128)(2,1)S(1)}, u32[]{:S(2)}, u32[]{:S(2)}) collective-permute-start(bf16[768,512]{1,0:T(8,128)(2,1)S(1)} %collective-permute-done.5), channel_id=1, source_target_pairs={{0,1},{1,2},{2,3},{3,4},{4,5},{5,6},{6,7},{7,0},{8,9},{9,10},{10,1... | collective-permute-start | bytes 2359304 | tf_op jit(solution)/shard_map/ppermute | solution.py:87
  80.6 11.1 %copy-start.13 = (bf16[4096,512]{1,0:T(8,128)(2,1)S(1)}, bf16[4096,512]{1,0:T(8,128)(2,1)}, u32[]{:S(2)}) copy-start(bf16[4096,512]{1,0:T(8,128)(2,1)} %param.11) | copy-start | bytes 12582916
  91.8 3.7 %copy-start.14 = (bf16[4096,512]{1,0:T(8,128)(2,1)S(1)}, bf16[4096,512]{1,0:T(8,128)(2,1)}, u32[]{:S(2)}) copy-start(bf16[4096,512]{1,0:T(8,128)(2,1)} %param.12) | copy-start | bytes 12582916
  99.8 0.7 copy-start.11
  103.6 18.6 %all-to-all-start = ((f32[16,4,512]{2,1,0:T(4,128)}), f32[16,4,512]{2,1,0:T(4,128)S(1)}, u32[]{:S(2)}, u32[]{:S(2)}) async-start(f32[16,4,512]{2,1,0:T(4,128)} %broadcast_in_dim.25), calls=%async_computation | async-start | bytes 262144 | tf_op jit(solution)/shard_map/all_to_all | solution.py:9
  116.5 1.3 copy-start.1
  120.2 1.7 copy-start.8
  124.1 19.1 %all-to-all-start.2 = ((f32[16,1,8192]{2,1,0:T(1,128)}), f32[16,1,8192]{2,1,0:T(1,128)S(1)}, u32[]{:S(2)}, u32[]{:S(2)}) async-start(f32[16,1,8192]{2,1,0:T(1,128)} %broadcast_in_dim.27), calls=%async_computation.2 | async-start | bytes 1048576 | tf_op jit(solution)/shard_map/all_to_all | solution.py:9
  133.9 35.7 %copy-start.15 = (f32[128]{0:T(128)S(1)}, f32[128]{0:T(128)}, u32[]{:S(2)}) copy-start(f32[128]{0:T(128)} %param.17) | copy-start | bytes 1540
  143.2 20.2 %all-to-all-start.1 = ((bf16[16,4,4,8,128]{4,3,2,1,0:T(8,128)(2,1)}), bf16[16,4,4,8,128]{4,3,2,1,0:T(8,128)(2,1)S(1)}, u32[]{:S(2)}, u32[]{:S(2)}) async-start(bf16[16,4,4,8,128]{4,3,2,1,0:T(8,128)(2,1)} %bitcast.68), calls=%async_computation.1 | async-start | bytes 1048576 | tf_op jit(solution)/shard_map/all_to_all | solution.py:42
  163.5 14.5 %copy-start.12 = (bf16[4,4,8,128]{3,2,1,0:T(8,128)(2,1)}, bf16[4,4,8,128]{3,2,1,0:T(8,128)(2,1)S(1)}, u32[]{:S(2)}) copy-start(bf16[4,4,8,128]{3,2,1,0:T(8,128)(2,1)S(1)} %reduce_sum.49) | copy-start | bytes 98308
  164.4 12.7 %all-to-all-start.3 = ((f32[16,4,4,128]{3,2,1,0:T(4,128)}), f32[16,4,4,128]{3,2,1,0:T(4,128)S(1)}, u32[]{:S(2)}, u32[]{:S(2)}) async-start(f32[16,4,4,128]{3,2,1,0:T(4,128)} %broadcast_in_dim.28), calls=%async_computation.3 | async-start | bytes 262144 | tf_op jit(solution)/shard_map/all_to_all | solution.py:9
